TPU v7x, 32 devices: a whole 2x2x4 slice. The times are simulated.
32 devices in a mesh: sp: 16 (over z, y, core), tp: 2 (over x).
Axes of the slice: x: 2, y: 2, z: 4, core: 2. Of those that a mesh axis runs over, the one named last changes fastest.
Arguments:
- latent: bfloat16 [8192, 2048], P(('sp', 'tp')), may hold values from -6 to 6
- context: bfloat16 [1024, 2048], P('sp'), may hold values from -6 to 6
- condition: float32 [2048], replicated, may hold values from -6 to 6
- context_condition: float32 [2048], replicated, may hold values from -6 to 6
- modulation_weight: bfloat16 [2048, 3, 2048], P('sp', None, 'tp'), may hold values from -0.125 to 0.125
- norm_gain: float32 [2048], replicated, may hold values from 0.1 to 1.9
- query_weight: bfloat16 [2048, 2048], P(None, 'tp'), may hold values from -0.125 to 0.125
- key_weight: bfloat16 [2048, 2048], P(None, 'tp'), may hold values from -0.125 to 0.125
- value_weight: bfloat16 [2048, 2048], P(None, 'tp'), may hold values from -0.125 to 0.125
- log_decay: float32 [2, 32], P(None, 'tp')
- head_gain: float32 [2048], P('tp'), may hold values from 0.1 to 1.9
- output_weight: bfloat16 [2048, 2048], P('sp'), may hold values from -0.125 to 0.125
Outputs:
- output: bfloat16 [8192, 2048], P(('sp', 'tp'))
All inputs are finite; a program needn't handle non-finite values.
Results may differ from a plain program's by a relative error of at most 0.0065.
Values may be sent and summed in bfloat16 or wider, within the bound.
A program may use at most 128 MiB of HBM per device.

v0:
```python
import functools

import jax
import jax.numpy as jnp
from jax import lax
from jax.experimental import pallas as pl
from jax.experimental.pallas import tpu as pltpu
from jax.sharding import PartitionSpec as P

HEAD = 64
CTX = 1024
LANES = 128
EPSILON = 1e-06
ROTARY_BASE = 10000.0
MESH = pl.DeviceIdType.MESH
F32 = jnp.float32
BF16 = jnp.bfloat16


def rotation_tables(positions):
    half_size = HEAD // 2
    frequency = 1.0 / ROTARY_BASE ** jnp.linspace(0.0, 1.0, half_size, dtype=F32)
    angles = positions[:, None] * frequency[None, :]
    cos, sin = jnp.cos(angles), jnp.sin(angles)
    return (
        jnp.concatenate([cos] * 4, axis=1),
        jnp.concatenate([-sin, sin, -sin, sin], axis=1),
    )


def dot(a, b, dims=((1,), (0,))):
    return lax.dot_general(a, b, (dims, ((), ())), preferred_element_type=F32)


def loop(count, body):
    def step(i, carry):
        body(i)
        return carry

    lax.fori_loop(0, count, step, 0)


def swap_halves(u, lane):
    return jnp.where(lane % HEAD < HEAD // 2, pltpu.roll(u, LANES - 32, 1), pltpu.roll(u, 32, 1))


def kernel(
    nsp,
    ntp,
    owned,
    latent,
    context,
    part,
    gain,
    wq,
    wk,
    wv,
    decay,
    row_decay,
    head_gain,
    wo_own,
    cos,
    sin,
    ccos,
    csin,
    out,
    lat,
    xn,
    cn,
    wq_v,
    wk_v,
    wv_v,
    wo,
    mrecv,
    mred,
    mod,
    modrow,
    q,
    k,
    v,
    ck,
    cv,
    st_send,
    st_recv,
    scan,
    en_send,
    en_recv,
    local,
    ret,
    got,
    acc,
    load_sem,
    lat_send_sem,
    lat_recv_sem,
    ms_sem,
    mr_sem,
    bs_sem,
    br_sem,
    ss_sem,
    sr_sem,
    es_sem,
    er_sem,
    gs_sem,
    gr_sem,
    wo_send_sem,
    wo_recv_sem,
):
    s = lax.axis_index("sp")
    t = lax.axis_index("tp")
    rows, dim = latent.shape
    tok = rows * ntp
    width = wq.shape[1]
    pairs = width // LANES
    crow = context.shape[0]
    nch = part.shape[0]
    owners = width // owned
    block = wo_own.shape[0]
    nz = nsp // 4
    z, y, c = s // 4, (s // 2) % 2, s % 2

    def remote(src, dst, send, recv, where):
        return pltpu.make_async_remote_copy(
            src_ref=src,
            dst_ref=dst,
            send_sem=send,
            recv_sem=recv,
            device_id=where,
            device_id_type=MESH,
        )

    loads = [
        pltpu.make_async_copy(latent, lat.at[t], load_sem.at[0]),
        pltpu.make_async_copy(wk, wk_v, load_sem.at[1]),
        pltpu.make_async_copy(wv, wv_v, load_sem.at[2]),
        pltpu.make_async_copy(wq, wq_v, load_sem.at[3]),
        pltpu.make_async_copy(wo_own, wo.at[s], load_sem.at[4]),
    ]

    def part_copy(j):
        return remote(part.at[j], mrecv.at[s], ms_sem.at[j], mr_sem.at[s], (j, t))

    for j in range(nch):
        @pl.when(s != j)
        def _():
            part_copy(j).start()

        @pl.when(s == j)
        def _():
            mrecv[j] = part[j]

    def lat_copy(d):
        peer = (t + d) % ntp
        return remote(latent, lat.at[t], lat_send_sem.at[d], lat_recv_sem.at[t], (s, peer))

    for d in range(1, ntp):
        lat_copy(d).start()
    for copy in loads:
        copy.start()

    def wo_copy(b, kind, src=None):
        if kind == 0:
            where = s + 4
        elif kind == 1:
            where = s - 4
        elif kind == 2:
            where = z * 4 + (1 - y) * 2 + c
        else:
            where = z * 4 + y * 2 + (1 - c)
        ref = wo.at[b] if src is None else src
        return remote(ref, wo.at[b], wo_send_sem.at[b, kind], wo_recv_sem.at[b], (where, t))

    def wo_arrived(b):
        remote(wo.at[b], wo.at[b], wo_send_sem.at[b, 0], wo_recv_sem.at[b], (s, t)).wait_recv()

    def up_ok(cond=True):
        return (z < nz - 1) & cond

    def wo_own_sends(act):
        @pl.when(z < nz - 1)
        def _():
            act(wo_copy(s, 0, wo_own))

        @pl.when(z > 0)
        def _():
            act(wo_copy(s, 1, wo_own))

        act(wo_copy(s, 2, wo_own))
        act(wo_copy(s, 3, wo_own))

    wo_own_sends(lambda copy: copy.start())

    def wo_y_arrived(distance):
        def one(zz):
            b = zz * 4 + (1 - y) * 2 + c
            wo_arrived(b)
            wo_copy(b, 3).start()

        if distance == 0:
            one(z)
            return

        @pl.when(z - distance >= 0)
        def _():
            one(z - distance)

        @pl.when(z + distance < nz)
        def _():
            one(z + distance)

    def wo_z_forward(distance, act, wait):
        @pl.when(z - distance >= 0)
        def _():
            b = s - 4 * distance
            if wait:
                wo_arrived(b)

            @pl.when(z < nz - 1)
            def _():
                act(wo_copy(b, 0))

            act(wo_copy(b, 2))
            act(wo_copy(b, 3))

        @pl.when(z + distance < nz)
        def _():
            b = s + 4 * distance
            if wait:
                wo_arrived(b)

            @pl.when(z > 0)
            def _():
                act(wo_copy(b, 1))

            act(wo_copy(b, 2))
            act(wo_copy(b, 3))

    def wo_step(distance):
        wo_z_forward(distance, lambda copy: copy.start(), True)

    def to_all(act):
        def one(i):
            where = (s + i // ntp) % nsp, (t + i % ntp) % ntp

            @pl.when(i > 0)
            def _():
                act(remote(mred, mod.at[t * nch + s], bs_sem.at[i], br_sem.at[t * nch + s], where))

        loop(nsp * ntp, one)

    @pl.when(s < nch)
    def _():
        def arrived(j):
            @pl.when(j != s)
            def _():
                remote(part.at[0], mrecv.at[j], ms_sem.at[0], mr_sem.at[j], (j, t)).wait_recv()

        loop(nsp, arrived)
        total = mrecv[0]
        for j in range(1, nsp):
            total = total + mrecv[j]
        mred[...] = total
        mod[t * nch + s] = total
        to_all(lambda copy: copy.start())

    for j in range(nch * ntp):
        @pl.when(t * nch + s != j)
        def _():
            remote(mred, mod.at[j], bs_sem.at[0], br_sem.at[j], (s, t)).wait_recv()

        @pl.when((t * nch + s == j) & (s >= nch))
        def _():
            remote(mred, mod.at[j], bs_sem.at[0], br_sem.at[j], (s, t)).wait_recv()

        modrow[:, j * LANES : (j + 1) * LANES] = mod[j]

    def normalise(src, dst, count, row):
        step = min(count, 64)

        def one(i):
            at = pl.ds(pl.multiple_of(i * step, step), step)
            x = src(at).astype(F32)
            inverse = lax.rsqrt(jnp.mean(x * x, axis=-1, keepdims=True) + EPSILON)
            dst[at, :] = (
                x * inverse * gain[...] * (1.0 + modrow[row + 1 : row + 2, :])
                + modrow[row : row + 1, :]
            ).astype(BF16)

        loop(count // step, one)

    lane_r = lax.broadcasted_iota(jnp.int32, (rows, LANES), 1)
    lane_c = lax.broadcasted_iota(jnp.int32, (crow, LANES), 1)
    tile = min(width, 256)

    normalise(lambda at: context[at, :], cn, crow, 3)
    loads[0].wait()
    loads[1].wait()
    loads[2].wait()

    def context_tile(j):
        at = pl.ds(pl.multiple_of(j * tile, tile), tile)
        kk = dot(cn[...], wk_v[:, at])
        cv[:, at] = dot(cn[...], wv_v[:, at]).astype(BF16)
        for h in range(tile // LANES):
            u = kk[:, h * LANES : (h + 1) * LANES]
            r = u * ccos[...] + swap_halves(u, lane_c) * csin[...]
            ck[:, pl.ds(pl.multiple_of(j * tile + h * LANES, LANES), LANES)] = r.astype(BF16)

    loop(width // tile, context_tile)
    loads[3].wait()

    def project(d):
        src = (t + d) % ntp
        here = pl.ds(pl.multiple_of(src * rows, rows), rows)

        @pl.when(d > 0)
        def _():
            remote(latent, lat.at[src], lat_send_sem.at[0], lat_recv_sem.at[src], (s, t)).wait_recv()

        normalise(lambda at: lat[src, at, :], xn, rows, 0)

        def tile_step(j):
            at = pl.ds(pl.multiple_of(j * tile, tile), tile)
            v[here, at] = dot(xn[...], wv_v[:, at]).astype(BF16)
            cc, sn = cos[here, :], sin[here, :]
            for w_v, dst, scale in ((wk_v, k, None), (wq_v, q, HEAD ** (-0.5))):
                full = dot(xn[...], w_v[:, at])
                for h in range(tile // LANES):
                    u = full[:, h * LANES : (h + 1) * LANES]
                    r = u * cc + swap_halves(u, lane_r) * sn
                    if scale is not None:
                        r = r * scale
                    dst[here, pl.ds(pl.multiple_of(j * tile + h * LANES, LANES), LANES)] = r.astype(
                        BF16
                    )

        loop(width // tile, tile_step)

    project(0)
    wo_y_arrived(0)
    for distance in range(1, nz // 2):
        wo_step(distance)
    if ntp > 1:
        loop(ntp - 1, lambda d: project(d + 1))
    for distance in range(max(nz // 2, 1), nz):
        wo_step(distance)
    for distance in range(1, nz // 2):
        wo_y_arrived(distance)

    row_s = lax.broadcasted_iota(jnp.int32, (LANES, LANES), 0)
    lane_s = lax.broadcasted_iota(jnp.int32, (LANES, LANES), 1)
    lane_1 = lax.broadcasted_iota(jnp.int32, (1, LANES), 1)
    time_t = lax.broadcasted_iota(jnp.int32, (tok, LANES), 0).astype(F32)
    time_c = lax.broadcasted_iota(jnp.int32, (crow, LANES), 0).astype(F32)

    def rate(direction, p):
        return jnp.where(lane_1 < HEAD, decay[direction, 2 * p], decay[direction, 2 * p + 1])

    def pack(forward, backward):
        return jnp.where(
            lane_s < HEAD,
            jnp.where(row_s < HEAD, forward, pltpu.roll(forward, HEAD, 1)),
            jnp.where(row_s < HEAD, pltpu.roll(backward, HEAD, 1), backward),
        ).astype(BF16)

    def states(p):
        at = pl.ds(pl.multiple_of(p * LANES, LANES), LANES)
        ahead, behind = rate(0, p), rate(1, p)
        for which, keys, values, time in ((0, k, v, time_t), (1, ck, cv, time_c)):
            length = time.shape[0]
            kk = keys[:, at].astype(F32)
            vv = values[:, at]
            weighted = (kk * jnp.exp(ahead * (length - 1.0 - time))).astype(BF16)
            forward = dot(weighted, vv, ((0,), (0,)))
            weighted = (kk * jnp.exp(behind * time)).astype(BF16)
            backward = dot(weighted, vv, ((0,), (0,)))
            packed = pack(forward, backward)
            for i in range(LANES // owned):
                st_send[p * (LANES // owned) + i, which] = packed[i * owned : (i + 1) * owned, :]

    loop(pairs, states)

    def state_copy(j):
        return remote(st_send.at[j], st_recv.at[s], ss_sem.at[j], sr_sem.at[s], (j, t))

    def send_states(d):
        j = (s + d) % nsp

        @pl.when((j < owners) & (d > 0))
        def _():
            state_copy(j).start()

    loop(nsp, send_states)

    @pl.when(s < owners)
    def _():
        st_recv[s] = st_send[s]

    row_q = lax.broadcasted_iota(jnp.int32, (tok, tok), 0)
    col_q = lax.broadcasted_iota(jnp.int32, (tok, tok), 1)
    lane_t = lax.broadcasted_iota(jnp.int32, (tok, LANES), 1)

    def inside(p):
        at = pl.ds(pl.multiple_of(p * LANES, LANES), LANES)
        qq, kk, vv = q[:, at], k[:, at], v[:, at]
        gap = (row_q - col_q).astype(F32)
        halves = []
        for a in range(2):
            ahead, behind = decay[0, 2 * p + a], decay[1, 2 * p + a]
            mine = (lane_t < HEAD) if a == 0 else (lane_t >= HEAD)
            scores = dot(jnp.where(mine, qq.astype(F32), 0.0).astype(BF16), kk, ((1,), (1,)))
            mask = jnp.where(gap == 0.0, 2.0, jnp.exp(jnp.where(gap > 0.0, ahead, -behind) * gap))
            halves.append(dot((scores * mask).astype(BF16), vv))
        local[:, at] = jnp.where(lane_t < HEAD, halves[0], halves[1])

    first = (pairs + 1) // 2
    loop(first, inside)

    lane_o = lax.broadcasted_iota(jnp.int32, (owned, LANES), 1)

    def enter_copy(j):
        return remote(en_send.at[j], en_recv.at[s], es_sem.at[j], er_sem.at[s], (j, t))

    @pl.when(s < owners)
    def _():
        def arrived(j):
            @pl.when(j != s)
            def _():
                remote(
                    st_send.at[0], st_recv.at[j], ss_sem.at[0], sr_sem.at[j], (j, t)
                ).wait_recv()

        loop(nsp, arrived)
        latent_step = jnp.exp(row_decay[...] * float(tok))
        context_step = jnp.exp(row_decay[...] * float(crow))

        def gather_forward(j, carry):
            return context_step * carry + st_recv[j, 1].astype(F32)

        def gather_backward(i, carry):
            return context_step * carry + st_recv[nsp - 1 - i, 1].astype(F32)

        zero = jnp.zeros((owned, LANES), F32)
        start = jnp.where(
            lane_o < HEAD,
            lax.fori_loop(0, nsp, gather_forward, zero),
            lax.fori_loop(0, nsp, gather_backward, zero),
        )

        def forward_step(i, carry):
            scan[i] = carry
            return latent_step * carry + st_recv[i, 0].astype(F32)

        lax.fori_loop(0, nsp, forward_step, start)

        def backward_step(n, carry):
            i = nsp - 1 - n
            en_send[i] = jnp.where(lane_o < HEAD, scan[i], carry).astype(BF16)
            return latent_step * carry + st_recv[i, 0].astype(F32)

        lax.fori_loop(0, nsp, backward_step, start)

        def send(j):
            @pl.when(j != s)
            def _():
                enter_copy(j).start()

        loop(nsp, send)
        en_recv[s] = en_send[s]

    loop(pairs - first, lambda p: inside(p + first))
    for distance in range(max(nz // 2, 1), nz):
        wo_y_arrived(distance)

    def entered(j):
        @pl.when(j != s)
        def _():
            remote(en_send.at[0], en_recv.at[j], es_sem.at[0], er_sem.at[j], (j, t)).wait_recv()

    loop(owners, entered)

    averaging = jnp.where((row_s < HEAD) == (lane_s < HEAD), 1.0 / HEAD, 0.0).astype(BF16)

    def head_mean(x):
        high = x.astype(BF16)
        low = (x - high.astype(F32)).astype(BF16)
        return dot(high, averaging) + dot(low, averaging)

    def ret_copy(d, p):
        peer = (t + d) % ntp
        at = pl.ds(pl.multiple_of(p * LANES, LANES), LANES)
        return remote(
            ret.at[pl.ds(pl.multiple_of(peer * rows, rows), rows), at],
            got.at[t, :, at],
            gs_sem.at[d, p],
            gr_sem.at[t, p],
            (s, peer),
        )

    def finish(p):
        at = pl.ds(pl.multiple_of(p * LANES, LANES), LANES)
        per = LANES // owned
        packed = jnp.concatenate([en_recv[p * per + i].astype(F32) for i in range(per)], axis=0)
        turned = pltpu.roll(packed, HEAD, 1)
        top = (row_s < HEAD) & (lane_s < HEAD)
        bottom = (row_s >= HEAD) & (lane_s >= HEAD)
        forward = jnp.where(top, packed, jnp.where(bottom, turned, 0.0)).astype(BF16)
        backward = jnp.where(top, turned, jnp.where(bottom, packed, 0.0)).astype(BF16)
        qq = q[:, at]
        o = (
            local[:, at]
            + dot(qq, forward) * jnp.exp(rate(0, p) * (time_t + 1.0))
            + dot(qq, backward) * jnp.exp(rate(1, p) * (float(tok) - time_t))
        )
        o = o - head_mean(o)
        spread = head_mean(o * o)
        ret[:, at] = (o * lax.rsqrt(spread + EPSILON) * head_gain[:, at]).astype(BF16)
        for d in range(1, ntp):
            ret_copy(d, p).start()
        got[t, :, at] = ret[pl.ds(pl.multiple_of(t * rows, rows), rows), at]

    loop(pairs, finish)

    for zz in range(nz):
        for yy in range(2):
            wo_arrived(zz * 4 + yy * 2 + (1 - c))
    loads[4].wait()

    per_head_block = width // block
    cols = min(dim, 512)

    def product(src, at):
        weight = wo[pl.ds(src * per_head_block, per_head_block), :, at]
        return dot(got[src], weight.reshape(width, cols))

    def own_product(n):
        at = pl.ds(pl.multiple_of(n * cols, cols), cols)
        acc[:, at] = product(t, at)

    loop(dim // cols, own_product)
    for d in range(1, ntp):
        src = (t + d) % ntp

        def got_wait(p):
            at = pl.ds(pl.multiple_of(p * LANES, LANES), LANES)
            remote(
                ret.at[pl.ds(0, rows), at],
                got.at[src, :, at],
                gs_sem.at[0, p],
                gr_sem.at[src, p],
                (s, t),
            ).wait_recv()

        loop(pairs, got_wait)
        last = d == ntp - 1

        def peer_product(n):
            at = pl.ds(pl.multiple_of(n * cols, cols), cols)
            total = acc[:, at] + product(src, at)
            if last:
                out[:, at] = (lat[t, :, at].astype(F32) + modrow[2:3, at] * total).astype(BF16)
            else:
                acc[:, at] = total

        loop(dim // cols, peer_product)

    for j in range(nch):
        @pl.when(s != j)
        def _():
            part_copy(j).wait_send()
    for d in range(1, ntp):
        lat_copy(d).wait_send()

    @pl.when(s < nch)
    def _():
        to_all(lambda copy: copy.wait_send())

    def states_left(d):
        j = (s + d) % nsp

        @pl.when((j < owners) & (d > 0))
        def _():
            state_copy(j).wait_send()

    loop(nsp, states_left)

    @pl.when(s < owners)
    def _():
        def left(j):
            @pl.when(j != s)
            def _():
                enter_copy(j).wait_send()

        loop(nsp, left)

    for d in range(1, ntp):
        loop(pairs, lambda p: ret_copy(d, p).wait_send())
    wo_own_sends(lambda copy: copy.wait_send())
    for distance in range(1, nz):
        wo_z_forward(distance, lambda copy: copy.wait_send(), False)
    for zz in range(nz):
        wo_copy(zz * 4 + (1 - y) * 2 + c, 3).wait_send()


def per_device(
    latent,
    context,
    condition,
    context_condition,
    modulation_weight,
    norm_gain,
    query_weight,
    key_weight,
    value_weight,
    log_decay,
    head_gain,
    output_weight,
):
    nsp, ntp = lax.axis_size("sp"), lax.axis_size("tp")
    s = lax.axis_index("sp")
    rows, dim = latent.shape
    tok = rows * ntp
    crow = context.shape[0]
    width = query_weight.shape[1]
    pairs = width // LANES
    owned = max(width // nsp, 16)
    owners = width // owned
    activated = jax.nn.silu(jnp.stack([condition, context_condition])).astype(BF16)
    entries, kinds, cols = modulation_weight.shape
    own_inputs = lax.dynamic_slice_in_dim(activated, s * entries, entries, 1)
    partial = jnp.einsum(
        "ce,erd->crd", own_inputs, modulation_weight, preferred_element_type=F32
    ).reshape(2 * kinds, cols)
    nch = cols // LANES
    part = jnp.pad(partial, ((0, 8 - 2 * kinds), (0, 0))).reshape(8, nch, LANES).transpose(1, 0, 2)
    cos, sin = rotation_tables(
        CTX + (s * tok).astype(F32) + jnp.arange(tok, dtype=F32)
    )
    ccos, csin = rotation_tables((s * crow).astype(F32) + jnp.arange(crow, dtype=F32))
    held = (s * owned + jnp.arange(owned)) // HEAD
    mine = jnp.take(log_decay, jnp.minimum(held, width // HEAD - 1), axis=1)
    row_decay = jnp.repeat(mine.T, HEAD, axis=1)
    vmem = pl.BlockSpec(memory_space=pltpu.VMEM)
    anywhere = pl.BlockSpec(memory_space=pl.ANY)
    smem = pl.BlockSpec(memory_space=pltpu.SMEM)
    dma = pltpu.SemaphoreType.DMA
    scratch = [
        pltpu.VMEM((ntp, rows, dim), BF16),
        pltpu.VMEM((rows, dim), BF16),
        pltpu.VMEM((crow, dim), BF16),
        pltpu.VMEM((dim, width), BF16),
        pltpu.VMEM((dim, width), BF16),
        pltpu.VMEM((dim, width), BF16),
        pltpu.VMEM((nsp,) + output_weight.shape, BF16),
        pltpu.VMEM((nsp, 8, LANES), F32),
        pltpu.VMEM((8, LANES), F32),
        pltpu.VMEM((ntp * nch, 8, LANES), F32),
        pltpu.VMEM((8, dim), F32),
        pltpu.VMEM((tok, width), BF16),
        pltpu.VMEM((tok, width), BF16),
        pltpu.VMEM((tok, width), BF16),
        pltpu.VMEM((crow, width), BF16),
        pltpu.VMEM((crow, width), BF16),
        pltpu.VMEM((owners, 2, owned, LANES), BF16),
        pltpu.VMEM((nsp, 2, owned, LANES), BF16),
        pltpu.VMEM((nsp, owned, LANES), F32),
        pltpu.VMEM((nsp, owned, LANES), BF16),
        pltpu.VMEM((owners, owned, LANES), BF16),
        pltpu.VMEM((tok, width), F32),
        pltpu.VMEM((tok, width), BF16),
        pltpu.VMEM((ntp, rows, width), BF16),
        pltpu.VMEM((rows, dim), F32),
        dma((5,)),
        dma((ntp,)),
        dma((ntp,)),
        dma((nch,)),
        dma((nsp,)),
        dma((nsp * ntp,)),
        dma((ntp * nch,)),
        dma((owners,)),
        dma((nsp,)),
        dma((nsp,)),
        dma((owners,)),
        dma((ntp, pairs)),
        dma((ntp, pairs)),
        dma((nsp, 4)),
        dma((nsp,)),
    ]
    return pl.pallas_call(
        functools.partial(kernel, nsp, ntp, owned),
        out_shape=jax.ShapeDtypeStruct((rows, dim), BF16),
        in_specs=[anywhere, vmem, vmem, vmem, anywhere, anywhere, anywhere, smem]
        + [vmem, vmem, anywhere]
        + [vmem] * 4,
        out_specs=vmem,
        scratch_shapes=scratch,
        compiler_params=pltpu.CompilerParams(
            has_side_effects=True, vmem_limit_bytes=66_000_000
        ),
    )(
        latent,
        context,
        part,
        norm_gain[None],
        query_weight,
        key_weight,
        value_weight,
        log_decay,
        row_decay,
        head_gain[None],
        output_weight,
        cos,
        sin,
        ccos,
        csin,
    )


def solution(mesh):
    in_specs = (
        P(("sp", "tp"), None),
        P("sp", None),
        P(),
        P(),
        P("sp", None, "tp"),
        P(),
        P(None, "tp"),
        P(None, "tp"),
        P(None, "tp"),
        P(None, "tp"),
        P("tp"),
        P("sp", None),
    )
    out_specs = P(("sp", "tp"), None)
    return jax.shard_map(
        per_device, mesh=mesh, in_specs=in_specs, out_specs=out_specs, check_vma=False
    )
```

profile of v0, /device:TPU:0, one launch (start us, length us, event | category | flops | bytes accessed | tf_op | source)
XLA Modules:
  0.0 122.9 jit_solution(16977529076772731650)
XLA Ops:
  0.0 0.0 copy-start
  0.1 0.1 fusion.5
  0.2 0.8 copy.17
  1.0 0.6 gather_fusion
  1.6 0.1 broadcast_select_fusion
  1.7 0.0 copy-done
  1.7 1.0 fusion.6
  2.7 0.6 pad_bitcast_fusion.part
  3.3 0.1 broadcast_in_dim.27
  3.4 0.7 reshape.95.row_decay
  4.1 0.2 fusion.1
  4.3 0.7 pad_maximum_fusion.2
  5.1 1.0 fusion
  6.1 1.3 %pad_maximum_fusion = (f32[512,128]{1,0:T(8,128)}, f32[512,128]{1,0:T(8,128)}) fusion(f32[512,32]{1,0:T(8,128)S(1)} %get-tuple-element.8, f32[512,32]{1,0:T(8,128)S(1)} %get-tuple-element.7, f32[512,32]{1,0:T(8,128)S(1)} %get-tuple-element.6), kind=kLoop, calls=%fused_computation.3 | loop fusion | flops 393216 | bytes 720896 | tf_op jit(solution)/shard_map/concatenate | solution.py:26
  7.3 113.2 %shard_map.118 = bf16[256,2048]{1,0:T(8,128)(2,1)} custom-call(bf16[256,2048]{1,0:T(8,128)(2,1)} %latent.1, bf16[64,2048]{1,0:T(8,128)(2,1)} %context.1, f32[8,8,128]{2,1,0:T(8,128)} %pad_bitcast_fusion.part, f32[1,2048]{1,0:T(1,128)} %bitcast.17, bf16[2048,1024]{1,0:T(8,128)(2,1)} %wq.1, bf16[2048,1024]{1,0:T(8,128)(2,1)} %wk.1, bf16[2048,1024]{1,0:T(8,128)(2,1)} %wv.1, ...), custom_call_target="tpu_custom_call" | custom-call | tf_op jit(solution)/shard_map/pallas_call | solution.py:688
  120.6 2.3 %copy.20 = bf16[256,2048]{1,0:T(8,128)(2,1)} copy(bf16[256,2048]{1,0:T(8,128)(2,1)} %shard_map.118) | data formatting | bytes 2097152
  (8 shorter events, 0.1 us)
Async XLA Ops:
  0.0 1.7 %copy-start = (bf16[128,3,1024]{2,0,1:T(8,128)(2,1)S(1)}, bf16[128,3,1024]{2,0,1:T(8,128)(2,1)}, u32[]{:S(2)}) copy-start(bf16[128,3,1024]{2,0,1:T(8,128)(2,1)} %param.18) | copy-start | bytes 2359300
where the time goes:
time: 123 us
  Pallas kernels  113 us (92%)
  local copies, waits for them, and re-layouts  5.22 us (4%)
  other arithmetic  3.41 us (3%)
    pallas_call x1, Pallas kernels, per_device(): pl.pallas_call(functools.partial(kernel, nsp, ntp, owned), out_shape=jax....  113 us
    unnamed x4, local copies, waits for them, and re-layouts  3.14 us

commit v1 on v0

--- a/solution.py
+++ b/solution.py
@@ -20,12 +20,10 @@
 def rotation_tables(positions):
     half_size = HEAD // 2
     frequency = 1.0 / ROTARY_BASE ** jnp.linspace(0.0, 1.0, half_size, dtype=F32)
-    angles = positions[:, None] * frequency[None, :]
-    cos, sin = jnp.cos(angles), jnp.sin(angles)
-    return (
-        jnp.concatenate([cos] * 4, axis=1),
-        jnp.concatenate([-sin, sin, -sin, sin], axis=1),
-    )
+    lane = jnp.arange(LANES)
+    angles = positions[:, None] * jnp.tile(frequency, LANES // half_size)[None, :]
+    sign = jnp.where(lane % HEAD < half_size, -1.0, 1.0).astype(F32)
+    return jnp.cos(angles), jnp.sin(angles) * sign[None, :]
 
 
 def dot(a, b, dims=((1,), (0,))):
@@ -56,13 +54,10 @@
     wk,
     wv,
     decay,
-    row_decay,
     head_gain,
     wo_own,
     cos,
     sin,
-    ccos,
-    csin,
     out,
     lat,
     xn,
@@ -148,12 +143,21 @@
         def _():
             mrecv[j] = part[j]
 
-    def lat_copy(d):
+    lead = rows // 4
+    pieces = (pl.ds(0, lead), pl.ds(lead, rows - lead))
+
+    def lat_copy(d, piece):
         peer = (t + d) % ntp
-        return remote(latent, lat.at[t], lat_send_sem.at[d], lat_recv_sem.at[t], (s, peer))
+        return remote(
+            latent.at[pieces[piece]],
+            lat.at[t, pieces[piece]],
+            lat_send_sem.at[d, piece],
+            lat_recv_sem.at[t, piece],
+            (s, peer),
+        )
 
     for d in range(1, ntp):
-        lat_copy(d).start()
+        lat_copy(d, 0).start()
     for copy in loads:
         copy.start()
 
@@ -172,9 +176,6 @@
     def wo_arrived(b):
         remote(wo.at[b], wo.at[b], wo_send_sem.at[b, 0], wo_recv_sem.at[b], (s, t)).wait_recv()
 
-    def up_ok(cond=True):
-        return (z < nz - 1) & cond
-
     def wo_own_sends(act):
         @pl.when(z < nz - 1)
         def _():
@@ -186,8 +187,6 @@
 
         act(wo_copy(s, 2, wo_own))
         act(wo_copy(s, 3, wo_own))
-
-    wo_own_sends(lambda copy: copy.start())
 
     def wo_y_arrived(distance):
         def one(zz):
@@ -207,35 +206,56 @@
         def _():
             one(z + distance)
 
-    def wo_z_forward(distance, act, wait):
-        @pl.when(z - distance >= 0)
-        def _():
-            b = s - 4 * distance
+    furthest = jnp.maximum(z, nz - 1 - z)
+
+    def wo_z_forward(distance, act, wait, late):
+        def one(b, kind, further):
             if wait:
                 wo_arrived(b)
 
-            @pl.when(z < nz - 1)
+            @pl.when(further)
             def _():
-                act(wo_copy(b, 0))
-
-            act(wo_copy(b, 2))
+                act(wo_copy(b, kind))
+
+            if late:
+                act(wo_copy(b, 2))
+            else:
+
+                @pl.when(furthest != distance)
+                def _():
+                    act(wo_copy(b, 2))
+
             act(wo_copy(b, 3))
 
+        @pl.when(z - distance >= 0)
+        def _():
+            one(s - 4 * distance, 0, z < nz - 1)
+
         @pl.when(z + distance < nz)
         def _():
-            b = s + 4 * distance
-            if wait:
+            one(s + 4 * distance, 1, z > 0)
+
+    def wo_step(distance):
+        wo_z_forward(distance, lambda copy: copy.start(), True, False)
+
+    def wo_late():
+        for b in (s - 4 * furthest, s + 4 * furthest):
+            @pl.when((b >= 0) & (b < nsp) & (furthest > 0))
+            def _():
+                wo_copy(b, 2).start()
+
+    def wo_y_early(distance):
+        @pl.when(furthest != distance)
+        def _():
+            wo_y_arrived(distance)
+
+    def wo_y_late():
+        for zz in (z - furthest, z + furthest):
+            @pl.when((zz >= 0) & (zz < nz) & (furthest > 0))
+            def _():
+                b = zz * 4 + (1 - y) * 2 + c
                 wo_arrived(b)
-
-            @pl.when(z > 0)
-            def _():
-                act(wo_copy(b, 1))
-
-            act(wo_copy(b, 2))
-            act(wo_copy(b, 3))
-
-    def wo_step(distance):
-        wo_z_forward(distance, lambda copy: copy.start(), True)
+                wo_copy(b, 3).start()
 
     def to_all(act):
         def one(i):
@@ -261,6 +281,10 @@
         mred[...] = total
         mod[t * nch + s] = total
         to_all(lambda copy: copy.start())
+
+    for d in range(1, ntp):
+        lat_copy(d, 1).start()
+    wo_own_sends(lambda copy: copy.start())
 
     for j in range(nch * ntp):
         @pl.when(t * nch + s != j)
@@ -302,7 +326,7 @@
         cv[:, at] = dot(cn[...], wv_v[:, at]).astype(BF16)
         for h in range(tile // LANES):
             u = kk[:, h * LANES : (h + 1) * LANES]
-            r = u * ccos[...] + swap_halves(u, lane_c) * csin[...]
+            r = u * cos[pl.ds(tok, crow), :] + swap_halves(u, lane_c) * sin[pl.ds(tok, crow), :]
             ck[:, pl.ds(pl.multiple_of(j * tile + h * LANES, LANES), LANES)] = r.astype(BF16)
 
     loop(width // tile, context_tile)
@@ -314,7 +338,14 @@
 
         @pl.when(d > 0)
         def _():
-            remote(latent, lat.at[src], lat_send_sem.at[0], lat_recv_sem.at[src], (s, t)).wait_recv()
+            for piece in range(2):
+                remote(
+                    latent.at[pieces[piece]],
+                    lat.at[src, pieces[piece]],
+                    lat_send_sem.at[0, piece],
+                    lat_recv_sem.at[src, piece],
+                    (s, t),
+                ).wait_recv()
 
         normalise(lambda at: lat[src, at, :], xn, rows, 0)
 
@@ -336,15 +367,14 @@
         loop(width // tile, tile_step)
 
     project(0)
+    near, mid = nz // 2, 3 * nz // 4
+    for distance in range(1, max(near, 1)):
+        wo_step(distance)
     wo_y_arrived(0)
-    for distance in range(1, nz // 2):
+    for distance in range(max(near, 1), max(mid, 1)):
         wo_step(distance)
     if ntp > 1:
         loop(ntp - 1, lambda d: project(d + 1))
-    for distance in range(max(nz // 2, 1), nz):
-        wo_step(distance)
-    for distance in range(1, nz // 2):
-        wo_y_arrived(distance)
 
     row_s = lax.broadcasted_iota(jnp.int32, (LANES, LANES), 0)
     lane_s = lax.broadcasted_iota(jnp.int32, (LANES, LANES), 1)
@@ -395,25 +425,41 @@
     def _():
         st_recv[s] = st_send[s]
 
-    row_q = lax.broadcasted_iota(jnp.int32, (tok, tok), 0)
-    col_q = lax.broadcasted_iota(jnp.int32, (tok, tok), 1)
-    lane_t = lax.broadcasted_iota(jnp.int32, (tok, LANES), 1)
+    gap = (row_s - lane_s).astype(F32)
+    count = tok // LANES
 
     def inside(p):
         at = pl.ds(pl.multiple_of(p * LANES, LANES), LANES)
-        qq, kk, vv = q[:, at], k[:, at], v[:, at]
-        gap = (row_q - col_q).astype(F32)
-        halves = []
+        kk, vv = k[:, at], v[:, at]
+        masks = []
         for a in range(2):
             ahead, behind = decay[0, 2 * p + a], decay[1, 2 * p + a]
-            mine = (lane_t < HEAD) if a == 0 else (lane_t >= HEAD)
-            scores = dot(jnp.where(mine, qq.astype(F32), 0.0).astype(BF16), kk, ((1,), (1,)))
-            mask = jnp.where(gap == 0.0, 2.0, jnp.exp(jnp.where(gap > 0.0, ahead, -behind) * gap))
-            halves.append(dot((scores * mask).astype(BF16), vv))
-        local[:, at] = jnp.where(lane_t < HEAD, halves[0], halves[1])
+            by_block = {0: jnp.where(gap == 0.0, 2.0, jnp.exp(jnp.where(gap > 0.0, ahead, -behind) * gap))}
+            ahead_step = jnp.exp(jnp.full((1, LANES), ahead * LANES, F32))
+            behind_step = jnp.exp(jnp.full((1, LANES), behind * LANES, F32))
+            for n in range(1, count):
+                if n == 1:
+                    by_block[1] = jnp.exp(ahead * (gap + LANES))
+                    by_block[-1] = jnp.exp(behind * (LANES - gap))
+                else:
+                    by_block[n] = by_block[n - 1] * ahead_step
+                    by_block[-n] = by_block[1 - n] * behind_step
+            masks.append(by_block)
+        for i in range(count):
+            here = slice(i * LANES, (i + 1) * LANES)
+            qq = q[here, at].astype(F32)
+            halves = []
+            for a in range(2):
+                mine = (lane_s < HEAD) if a == 0 else (lane_s >= HEAD)
+                scores = dot(jnp.where(mine, qq, 0.0).astype(BF16), kk, ((1,), (1,)))
+                mask = jnp.concatenate([masks[a][i - j] for j in range(count)], axis=1)
+                halves.append(dot((scores * mask).astype(BF16), vv))
+            local[here, at] = jnp.where(lane_s < HEAD, halves[0], halves[1])
 
     first = (pairs + 1) // 2
     loop(first, inside)
+    for distance in range(1, max(near, 1)):
+        wo_y_early(distance)
 
     lane_o = lax.broadcasted_iota(jnp.int32, (owned, LANES), 1)
 
@@ -430,8 +476,10 @@
                 ).wait_recv()
 
         loop(nsp, arrived)
-        latent_step = jnp.exp(row_decay[...] * float(tok))
-        context_step = jnp.exp(row_decay[...] * float(crow))
+        head = s * owned // HEAD
+        rates = jnp.where(lane_o < HEAD, decay[0, head], decay[1, head])
+        latent_step = jnp.exp(rates * float(tok))
+        context_step = jnp.exp(rates * float(crow))
 
         def gather_forward(j, carry):
             return context_step * carry + st_recv[j, 1].astype(F32)
@@ -467,9 +515,12 @@
         loop(nsp, send)
         en_recv[s] = en_send[s]
 
+    for distance in range(max(mid, 1), nz):
+        wo_step(distance)
+    wo_late()
     loop(pairs - first, lambda p: inside(p + first))
-    for distance in range(max(nz // 2, 1), nz):
-        wo_y_arrived(distance)
+    for distance in range(max(near, 1), nz):
+        wo_y_early(distance)
 
     def entered(j):
         @pl.when(j != s)
@@ -520,6 +571,7 @@
 
     loop(pairs, finish)
 
+    wo_y_late()
     for zz in range(nz):
         for yy in range(2):
             wo_arrived(zz * 4 + yy * 2 + (1 - c))
@@ -568,7 +620,8 @@
         def _():
             part_copy(j).wait_send()
     for d in range(1, ntp):
-        lat_copy(d).wait_send()
+        lat_copy(d, 0).wait_send()
+        lat_copy(d, 1).wait_send()
 
     @pl.when(s < nch)
     def _():
@@ -596,7 +649,7 @@
         loop(pairs, lambda p: ret_copy(d, p).wait_send())
     wo_own_sends(lambda copy: copy.wait_send())
     for distance in range(1, nz):
-        wo_z_forward(distance, lambda copy: copy.wait_send(), False)
+        wo_z_forward(distance, lambda copy: copy.wait_send(), False, True)
     for zz in range(nz):
         wo_copy(zz * 4 + (1 - y) * 2 + c, 3).wait_send()
 
@@ -632,13 +685,9 @@
     ).reshape(2 * kinds, cols)
     nch = cols // LANES
     part = jnp.pad(partial, ((0, 8 - 2 * kinds), (0, 0))).reshape(8, nch, LANES).transpose(1, 0, 2)
-    cos, sin = rotation_tables(
-        CTX + (s * tok).astype(F32) + jnp.arange(tok, dtype=F32)
-    )
-    ccos, csin = rotation_tables((s * crow).astype(F32) + jnp.arange(crow, dtype=F32))
-    held = (s * owned + jnp.arange(owned)) // HEAD
-    mine = jnp.take(log_decay, jnp.minimum(held, width // HEAD - 1), axis=1)
-    row_decay = jnp.repeat(mine.T, HEAD, axis=1)
+    place = jnp.arange(tok + crow)
+    place = jnp.where(place < tok, CTX + s * tok + place, s * crow + place - tok)
+    cos, sin = rotation_tables(place.astype(F32))
     vmem = pl.BlockSpec(memory_space=pltpu.VMEM)
     anywhere = pl.BlockSpec(memory_space=pl.ANY)
     smem = pl.BlockSpec(memory_space=pltpu.SMEM)
@@ -670,8 +719,8 @@
         pltpu.VMEM((ntp, rows, width), BF16),
         pltpu.VMEM((rows, dim), F32),
         dma((5,)),
-        dma((ntp,)),
-        dma((ntp,)),
+        dma((ntp, 2)),
+        dma((ntp, 2)),
         dma((nch,)),
         dma((nsp,)),
         dma((nsp * ntp,)),
@@ -689,8 +738,7 @@
         functools.partial(kernel, nsp, ntp, owned),
         out_shape=jax.ShapeDtypeStruct((rows, dim), BF16),
         in_specs=[anywhere, vmem, vmem, vmem, anywhere, anywhere, anywhere, smem]
-        + [vmem, vmem, anywhere]
-        + [vmem] * 4,
+        + [vmem, anywhere, vmem, vmem],
         out_specs=vmem,
         scratch_shapes=scratch,
         compiler_params=pltpu.CompilerParams(
@@ -705,13 +753,10 @@
         key_weight,
         value_weight,
         log_decay,
-        row_decay,
         head_gain[None],
         output_weight,
         cos,
         sin,
-        ccos,
-        csin,
     )
 
 

time: 123 us -> 97.5 us (0.79)
  Pallas kernels: 113 us -> 90.3 us
  other arithmetic: 3.41 us -> 2.03 us
  local copies, waits for them, and re-layouts: 5.22 us -> 3.97 us
    pallas_call x1, Pallas kernels: 113 us -> 90.3 us  [per_device(): pl.pallas_call(functools.partial(kernel, nsp, ntp, owned), out_shape=jax....]
    concatenate x2 -> x0, other arithmetic: 2.01 us -> none  [rotation_tables(): jnp.concatenate([cos] * 4, axis=1)]
    mul x0 -> x1, other arithmetic: none -> 1.92 us  [rotation_tables(): return (jnp.cos(angles), jnp.sin(angles) * sign[None, :])]
    unnamed x4 -> x3, local copies, waits for them, and re-layouts: 3.14 us -> 3.25 us
where the time goes in v1:
time: 97.5 us; the launch traced here: 97.3 us
  Pallas kernels  90.3 us (93%)
  local copies, waits for them, and re-layouts  3.97 us (4%)
  other arithmetic  2.03 us (2%)
    pallas_call x1, Pallas kernels, per_device(): pl.pallas_call(functools.partial(kernel, nsp, ntp, owned), out_shape=jax....  90.3 us
    unnamed x3, local copies, waits for them, and re-layouts  3.25 us

profile of v1, /device:TPU:0, one launch (start us, length us, event | category | flops | bytes accessed | tf_op | source)
XLA Modules:
  0.0 97.3 jit_solution(14099898647980112140)
XLA Ops:
  0.0 0.0 copy-start
  0.0 0.1 fusion.3
  0.1 0.1 mul.65
  0.2 0.9 copy-done
  1.1 0.9 fusion.4
  2.1 0.6 pad_bitcast_fusion.part
  2.7 1.9 %fusion = (f32[576,128]{1,0:T(8,128)}, f32[576,128]{1,0:T(8,128)}) fusion(f32[128]{0:T(128)S(1)} %compare_select_fusion, f32[128]{0:T(128)S(1)} %mul.65, f32[576]{0:T(1024)S(1)} %select_convert_fusion), kind=kLoop, calls=%fused_computation.2 | loop fusion | flops 147456 | bytes 593152 | tf_op jit(solution)/shard_map/mul | solution.py:26
  4.7 90.3 %shard_map.118 = bf16[256,2048]{1,0:T(8,128)(2,1)} custom-call(bf16[256,2048]{1,0:T(8,128)(2,1)} %latent.1, bf16[64,2048]{1,0:T(8,128)(2,1)} %context.1, f32[8,8,128]{2,1,0:T(8,128)} %pad_bitcast_fusion.part, f32[1,2048]{1,0:T(1,128)} %bitcast.14, bf16[2048,1024]{1,0:T(8,128)(2,1)} %wq.1, bf16[2048,1024]{1,0:T(8,128)(2,1)} %wk.1, bf16[2048,1024]{1,0:T(8,128)(2,1)} %wv.1, ...), custom_call_target="tpu_custom_call" | custom-call | tf_op jit(solution)/shard_map/pallas_call | solution.py:737
  95.0 2.3 %copy.15 = bf16[256,2048]{1,0:T(8,128)(2,1)} copy(bf16[256,2048]{1,0:T(8,128)(2,1)} %shard_map.118) | data formatting | bytes 2097152
  (6 shorter events, 0.1 us)
Async XLA Ops:
  0.0 1.1 %copy-start = (bf16[128,3,1024]{2,0,1:T(8,128)(2,1)S(1)}, bf16[128,3,1024]{2,0,1:T(8,128)(2,1)}, u32[]{:S(2)}) copy-start(bf16[128,3,1024]{2,0,1:T(8,128)(2,1)} %param.16) | copy-start | bytes 2359300

commit v2 on v1

--- a/solution.py
+++ b/solution.py
@@ -572,12 +572,14 @@
     loop(pairs, finish)
 
     wo_y_late()
-    for zz in range(nz):
-        for yy in range(2):
-            wo_arrived(zz * 4 + yy * 2 + (1 - c))
     loads[4].wait()
-
     per_head_block = width // block
+
+    def weight_rows(src):
+        for i in range(per_head_block // 2):
+            wo_arrived(src * per_head_block + 2 * i + (1 - c))
+
+    weight_rows(t)
     cols = min(dim, 512)
 
     def product(src, at):
@@ -602,6 +604,7 @@
                 (s, t),
             ).wait_recv()
 
+        weight_rows(src)
         loop(pairs, got_wait)
         last = d == ntp - 1
 

time: 97.5 us -> 97.5 us (level)
  no operation moved by 1% of the time
where the time goes in v2:
time: 97.5 us; the launch traced here: 97.3 us
  Pallas kernels  90.3 us (93%)
  local copies, waits for them, and re-layouts  3.97 us (4%)
  other arithmetic  2.03 us (2%)
    pallas_call x1, Pallas kernels, per_device(): pl.pallas_call(functools.partial(kernel, nsp, ntp, owned), out_shape=jax....  90.3 us
    unnamed x3, local copies, waits for them, and re-layouts  3.25 us

profile of v2, /device:TPU:0, one launch (start us, length us, event | category | flops | bytes accessed | tf_op | source)
XLA Modules:
  0.0 97.3 jit_solution(17223950247982453962)
XLA Ops:
  0.0 0.0 copy-start
  0.0 0.1 fusion.3
  0.1 0.1 mul.65
  0.2 0.9 copy-done
  1.1 0.9 fusion.4
  2.1 0.6 pad_bitcast_fusion.part
  2.7 1.9 %fusion = (f32[576,128]{1,0:T(8,128)}, f32[576,128]{1,0:T(8,128)}) fusion(f32[128]{0:T(128)S(1)} %compare_select_fusion, f32[128]{0:T(128)S(1)} %mul.65, f32[576]{0:T(1024)S(1)} %select_convert_fusion), kind=kLoop, calls=%fused_computation.2 | loop fusion | flops 147456 | bytes 593152 | tf_op jit(solution)/shard_map/mul | solution.py:26
  4.7 90.3 %shard_map.118 = bf16[256,2048]{1,0:T(8,128)(2,1)} custom-call(bf16[256,2048]{1,0:T(8,128)(2,1)} %latent.1, bf16[64,2048]{1,0:T(8,128)(2,1)} %context.1, f32[8,8,128]{2,1,0:T(8,128)} %pad_bitcast_fusion.part, f32[1,2048]{1,0:T(1,128)} %bitcast.14, bf16[2048,1024]{1,0:T(8,128)(2,1)} %wq.1, bf16[2048,1024]{1,0:T(8,128)(2,1)} %wk.1, bf16[2048,1024]{1,0:T(8,128)(2,1)} %wv.1, ...), custom_call_target="tpu_custom_call" | custom-call | tf_op jit(solution)/shard_map/pallas_call | solution.py:740
  95.0 2.3 %copy.15 = bf16[256,2048]{1,0:T(8,128)(2,1)} copy(bf16[256,2048]{1,0:T(8,128)(2,1)} %shard_map.118) | data formatting | bytes 2097152
  (6 shorter events, 0.1 us)
Async XLA Ops:
  0.0 1.1 %copy-start = (bf16[128,3,1024]{2,0,1:T(8,128)(2,1)S(1)}, bf16[128,3,1024]{2,0,1:T(8,128)(2,1)}, u32[]{:S(2)}) copy-start(bf16[128,3,1024]{2,0,1:T(8,128)(2,1)} %param.16) | copy-start | bytes 2359300
